TPU v7x, 32 devices: a whole 2x2x4 slice. The times are simulated.
32 devices in a mesh: sp: 8 (over z, x), tp: 4 (over y, core).
Axes of the slice: x: 2, y: 2, z: 4, core: 2. Of those that a mesh axis runs over, the one named last changes fastest.
Arguments:
- tokens: bfloat16 [4096, 4096], P('sp', 'tp'), may hold values from -8 to 8
- w_key: bfloat16 [4096, 2048], P(None, 'tp'), may hold values from -0.09375 to 0.09375
- w_value: bfloat16 [4096, 2048], P(None, 'tp'), may hold values from -0.09375 to 0.09375
- w_beta: bfloat16 [4096, 16], replicated, may hold values from -0.09375 to 0.09375
- w_decay: bfloat16 [4096, 16], replicated, may hold values from -0.09375 to 0.09375
- beta_bias: float32 [16], replicated, may hold values from -6 to -4
- decay_rate: float32 [16], replicated, as said below
- forgetting_increment: float32 [16, 4096], P('tp', 'sp')
- new_query: bfloat16 [16, 128], P('tp', 'sp'), may hold values from -6 to 6
- read_gain: bfloat16 [128], replicated, may hold values from 0.099609375 to 1.8984375
Outputs:
- state_cache: bfloat16 [16, 128, 128], P('tp', 'sp')
- first_read: float32 [16, 128], P('tp')
Inputs may be any that keep to these rules, and one draw needn't show every extreme that they name: `decay_rate`: positive.
All inputs are finite; a program needn't handle non-finite values.
Results may differ from a plain program's by a relative error of at most 0.0075.
Values may be sent and summed in bfloat16 or wider, within the bound.
A program may use at most 64 MiB of HBM per device.

v0:
```python
import jax
import jax.numpy as jnp
from jax import lax
from jax.sharding import PartitionSpec as P

DK = 128
DV = 128
BLOCK = 64
norm_eps = 1e-06


def prefix(part, axis, combine, identity):
    count = lax.axis_size(axis)
    place = lax.axis_index(axis)
    ahead = count - 1 - place
    gathered = lax.all_gather(part, axis)
    state = jnp.zeros_like(part) + jnp.asarray(identity, part.dtype)

    def one(lap, state):
        source = count - 1 - lap
        return combine(state, lax.dynamic_index_in_dim(gathered, source, 0, False))

    return lax.fori_loop(0, ahead, one, state)


def matmul_f32(left, right):
    return jnp.dot(left, right, precision=lax.Precision.HIGHEST)


def batched_f32(left, right):
    return jnp.einsum("hij,hjk->hik", left, right, precision=lax.Precision.HIGHEST)


def unit_inverse(lower):
    current_size = lower.shape[0]
    identity = jnp.eye(current_size, dtype=jnp.float32)
    result = identity - lower
    lower_power = lower
    covered = 2
    while covered < current_size:
        lower_power = matmul_f32(lower_power, lower_power)
        result = matmul_f32(result, identity + lower_power)
        covered = covered * 2
    return result


def block_terms(key_blk, value_blk, beta_blk, logd_blk):
    current_size = key_blk.shape[0]
    cumulative = jnp.cumsum(logd_blk)
    spread = cumulative[:, None] - cumulative[None, :]
    location_positions = jnp.arange(current_size)
    causal = location_positions[:, None] >= location_positions[None, :]
    strict = location_positions[:, None] > location_positions[None, :]
    decay_table = jnp.where(causal, jnp.exp(jnp.where(causal, spread, 0.0)), 0.0)
    key_beta = key_blk * beta_blk[:, None]
    lower = jnp.where(strict, matmul_f32(key_beta, key_blk.T) * decay_table, 0.0)
    inverse = unit_inverse(lower)
    update = matmul_f32(inverse, value_blk * beta_blk[:, None])
    erase = matmul_f32(inverse, key_beta * jnp.exp(cumulative)[:, None])
    key_remainder = key_blk * jnp.exp(cumulative[-1] - cumulative)[:, None]
    return (update, erase, key_remainder, jnp.exp(cumulative[-1]))


def per_device(
    tokens,
    w_key,
    w_value,
    w_beta,
    w_decay,
    beta_bias,
    decay_rate,
    forgetting_increment,
    new_query,
    read_gain,
):
    heads_here = w_key.shape[1] // DK
    token_count = tokens.shape[0]
    head_start = lax.axis_index("tp") * heads_here
    gate_weights = jnp.concatenate(
        [
            lax.dynamic_slice_in_dim(w_beta, head_start, heads_here, 1),
            lax.dynamic_slice_in_dim(w_decay, head_start, heads_here, 1),
        ],
        axis=1,
    )
    piece = lax.all_gather(tokens, "tp", axis=1, tiled=True)
    key_acc = jnp.dot(piece, w_key, preferred_element_type=jnp.float32)
    value_acc = jnp.dot(piece, w_value, preferred_element_type=jnp.float32)
    gate_acc = jnp.dot(piece, gate_weights, preferred_element_type=jnp.float32)
    key_wide = (
        lax.optimization_barrier(key_acc.astype(jnp.bfloat16))
        .astype(jnp.float32)
        .reshape(token_count, heads_here, DK)
    )
    key_unit = key_wide * lax.rsqrt(jnp.sum(key_wide * key_wide, axis=-1, keepdims=True) + norm_eps)
    value_wide = (
        lax.optimization_barrier(value_acc.astype(jnp.bfloat16))
        .astype(jnp.float32)
        .reshape(token_count, heads_here, DV)
    )
    bias_here = lax.dynamic_slice_in_dim(beta_bias, head_start, heads_here, 0)
    rate_here = lax.dynamic_slice_in_dim(decay_rate, head_start, heads_here, 0)
    beta = jax.nn.sigmoid(gate_acc[:, :heads_here] + bias_here).T
    log_decay = (
        -rate_here[:, None] * jax.nn.softplus(gate_acc[:, heads_here:].T) + forgetting_increment
    )
    blocks = token_count // BLOCK
    key_heads = key_unit.transpose(1, 0, 2).reshape(heads_here, blocks, BLOCK, DK)
    value_heads = value_wide.transpose(1, 0, 2).reshape(heads_here, blocks, BLOCK, DV)
    terms = jax.vmap(jax.vmap(block_terms))(
        key_heads,
        value_heads,
        beta.reshape(heads_here, blocks, BLOCK),
        log_decay.reshape(heads_here, blocks, BLOCK),
    )
    inputs = tuple((jnp.moveaxis(item, 1, 0) for item in terms))
    identity = jnp.broadcast_to(jnp.eye(DK, dtype=jnp.float32), (heads_here, DK, DK))
    value_zeros = jnp.zeros((heads_here, DK, DV), jnp.float32)
    padding = jnp.zeros((heads_here, BLOCK, DK), jnp.float32)

    def advance(state, block_in):
        update, erase, key_remainder, keep = block_in
        fresh = jnp.concatenate([update, padding], axis=-1) - jnp.einsum(
            "hcd,hde->hce", erase, state, precision=lax.Precision.HIGHEST
        )
        state = keep[:, None, None] * state + jnp.einsum(
            "hcd,hce->hde", key_remainder, fresh, precision=lax.Precision.HIGHEST
        )
        return (state, None)

    combined, _ = lax.scan(advance, jnp.concatenate([value_zeros, identity], axis=-1), inputs)
    local_b = combined[:, :, :DV]
    local_left = combined[:, :, DV:]
    later_product = prefix(local_left, "sp", batched_f32, identity)
    summed = lax.psum_scatter(
        batched_f32(later_product, local_b), "sp", scatter_dimension=1, tiled=True
    )
    own_rows = summed.astype(jnp.bfloat16)
    partial_read = jnp.sum(
        new_query.astype(jnp.float32)[:, :, None] * own_rows.astype(jnp.float32), axis=1
    )
    raw_read = lax.psum(partial_read, "sp")
    first_read = (
        raw_read
        * lax.rsqrt(jnp.mean(raw_read * raw_read, axis=-1, keepdims=True) + norm_eps)
        * read_gain.astype(jnp.float32)
    )
    return (own_rows, first_read)


def solution(mesh):
    return jax.shard_map(
        per_device,
        mesh=mesh,
        in_specs=(
            P("sp", "tp"),
            P(None, "tp"),
            P(None, "tp"),
            P(),
            P(),
            P(),
            P(),
            P("tp", "sp"),
            P("tp", "sp"),
            P(),
        ),
        out_specs=(P("tp", "sp", None), P("tp", None)),
        check_vma=False,
    )
```

profile of v0, /device:TPU:0, one launch (start us, length us, event | category | flops | bytes accessed | tf_op | source)
XLA Modules:
  0.0 263.8 jit_solution(13869263426340788410)
XLA Ops:
  11.1 35.6 %all-gather.4.cloned.1.call-done = bf16[512,4096]{1,0:T(8,128)(2,1)} async-done(((bf16[512,1024]{1,0:T(8,128)(2,1)}), bf16[512,4096]{1,0:T(8,128)(2,1)}) %all-gather.4.cloned.1.call-update) | async-done | bytes 4194320 | tf_op jit(solution)/shard_map/all_gather | solution.py:86
  46.8 3.4 %convolution_bitcast_fusion.3 = f32[512,8]{0,1:T(8,128)S(1)} fusion(bf16[512,4096]{1,0:T(8,128)(2,1)} %all-gather.4.cloned.1.call-done, bf16[4096,4]{0,1:T(4,128)(2,1)S(1)} %get-tuple-element.148, bf16[4096,4]{0,1:T(4,128)(2,1)S(1)} %get-tuple-element.149), kind=kOutput, calls=%fused_computation.25 | convolution fusion | flops 33685504 | bytes 4276224 | tf_op jit(solution)/shard_map/dot_general | solution.py:89
  52.9 5.9 %convolution_convert_fusion.1 = bf16[512,512]{1,0:T(8,128)(2,1)S(1)} fusion(bf16[512,4096]{1,0:T(8,128)(2,1)} %all-gather.4.cloned.1.call-done, bf16[4096,512]{1,0:T(8,128)(2,1)} %param.15), kind=kOutput, calls=%fused_computation.24 | convolution fusion | flops 2147745792 | bytes 8912896 | tf_op jit(solution)/shard_map/dot_general | solution.py:87
  58.8 2.3 convolution_convert_fusion
  62.7 2.1 multiply_bitcast_fusion
  64.7 2.7 %fusion.15 = f32[4,8,64,64]{3,2,1,0:T(8,128)S(1)} fusion(f32[4,8,64,128]{3,2,1,0:T(8,128)S(1)} %bitcast.101, f32[4,8,64]{2,1,0:T(8,128)S(1)} %reduce_window_sum.11, f32[4,8,64]{2,1,0:T(8,128)S(1)} %mul.102, pred[64,64]{1,0:T(8,128)(4,1)} %get-tuple-element.150, pred[64,64]{1,0:T(8,128)(4,1)} %get-tuple-element.151), kind=kOutput, calls=%fused_computation.22 | convolution fusion | flops 202244096 | bytes 1597440 | tf_op jit(solution)/shard_map/vmap(vmap())/dot_general | solution.py:27
  72.2 1.4 fusion.23
  79.6 2.6 convolution_bitcast_fusion.1
  83.5 29.7 %while.22 = (s32[]{:T(128)}, f32[4,128,256]{2,1,0:T(8,128)S(1)}, f32[8,4]{1,0:T(8,128)}, f32[8,4,64,128]{3,2,0,1:T(8,128)}, f32[8,4,64,128]{3,2,0,1:T(8,128)S(1)}, /*index=5*/f32[8,4,64,128]{3,2,0,1:T(8,128)}, s32[]{:T(128)}) while((s32[]{:T(128)}, f32[4,128,256]{2,1,0:T(8,128)S(1)}, f32[8,4]{1,0:T(8,128)}, f32[8,4,64,128]{3,2,0,1:T(8,128)}, ...), condition=%wide.region_3.4_spmd, body=%wide.region_2.3_spmd.sunk | while | flops 201654272 | bytes 2752661 | solution.py:131
  84.2 1.3 convolution_subtract_fusion.2
  85.5 1.7 convolution_add_fusion.3
  87.9 1.3 convolution_subtract_fusion.2
  89.2 1.7 convolution_add_fusion.3
  91.6 1.3 convolution_subtract_fusion.2
  92.9 1.7 convolution_add_fusion.3
  96.7 1.7 convolution_add_fusion.3
  100.4 1.7 convolution_add_fusion.3
  104.1 1.7 convolution_add_fusion.3
  107.8 1.7 convolution_add_fusion.3
  111.5 1.7 convolution_add_fusion.3
  114.0 49.2 %all-gather.6.cloned.1.call-done = f32[32,128,128]{2,1,0:T(8,128)} async-done(((f32[4,128,128]{2,1,0:T(8,128)}), f32[32,128,128]{2,1,0:T(8,128)}) %all-gather.6.cloned.1.call-update) | async-done | bytes 2097168 | tf_op jit(solution)/shard_map/all_gather | solution.py:16
  163.2 11.3 %while.23 = (s32[]{:T(128)}, f32[4,128,128]{1,2,0:T(8,128)S(1)}, s32[]{:T(128)}, f32[8,4,128,128]{3,2,1,0:T(8,128)}, s32[]{:T(128)}, /*index=5*/s32[]{:T(128)}, s32[]{:T(128)}, s32[]{:T(128)}) while((s32[]{:T(128)}, f32[4,128,128]{1,2,0:T(8,128)S(1)}, s32[]{:T(128)}, f32[8,4,128,128]{3,2,1,0:T(8,128)}, s32[]{:T(128)}, /*index=5*/s32[]{:T(128)}, ...), condition=%wide.region_5.6_spmd, body=%wide.region_4.5_spmd.sunk | while | flops 100663304 | bytes 1310863 | solution.py:23
  163.3 1.6 convolution_bitcast_fusion.5
  164.9 1.6 convolution_bitcast_fusion.5
  166.5 1.6 convolution_bitcast_fusion.5
  168.1 1.6 convolution_bitcast_fusion.5
  169.7 1.6 convolution_bitcast_fusion.5
  171.3 1.6 convolution_bitcast_fusion.5
  172.9 1.6 convolution_bitcast_fusion.5
  175.9 59.9 %reduce-scatter.2.cloned.1.call-done = f32[4,16,128]{2,1,0:T(8,128)} async-done(((f32[4,128,128]{2,1,0:T(8,128)}), f32[4,16,128]{2,1,0:T(8,128)}) %reduce-scatter.2.cloned.1.call-update) | async-done | bytes 32784 | tf_op jit(solution)/shard_map/reduce_scatter | solution.py:135
  235.7 1.4 multiply_reduce_fusion.1
  237.1 19.4 %psum.7 = f32[4,128]{1,0:T(4,128)S(1)} all-reduce(f32[4,128]{1,0:T(4,128)S(1)} %get-tuple-element.144), channel_id=1, replica_groups=mesh['sp'=8,'tp'=4] {'sp'}, use_global_device_ids=true, to_apply=%region_8.9 | all-reduce | flops 512 | bytes 4096 | tf_op jit(solution)/shard_map/psum | solution.py:142
  (86 shorter events, 35.4 us)
Async XLA Ops:
  7.2 43.0 %copy-start.1 = (f32[4,512]{1,0:T(4,128)S(1)}, f32[4,512]{1,0:T(4,128)}, u32[]{:S(2)}) copy-start(f32[4,512]{1,0:T(4,128)} %param.21) | copy-start | bytes 24580
  7.2 39.6 %all-gather.4.cloned.1.call-start = ((), (), s32[]{:S(2)}) async-start(), calls=%async_computation.1 | async-start | bytes 5242880 | tf_op jit(solution)/shard_map/all_gather | solution.py:86
  7.9 155.3 %all-gather.6.cloned.1.call-start = ((), (), s32[]{:S(2)}) async-start(), calls=%async_computation.3 | async-start | bytes 2359296 | tf_op jit(solution)/shard_map/all_gather | solution.py:16
  52.9 5.9 %copy-start = (bf16[512,4096]{1,0:T(8,128)(2,1)S(1)}, bf16[512,4096]{1,0:T(8,128)(2,1)}, u32[]{:S(2)}) copy-start(bf16[512,4096]{1,0:T(8,128)(2,1)} %all-gather.4.cloned.1.call-done) | copy-start | bytes 12582916
  52.9 5.9 %copy-start.3 = (bf16[4096,512]{1,0:T(8,128)(2,1)S(1)}, bf16[4096,512]{1,0:T(8,128)(2,1)}, u32[]{:S(2)}) copy-start(bf16[4096,512]{1,0:T(8,128)(2,1)} %param.16) | copy-start | bytes 12582916
  113.9 61.9 %copy-start.4 = (bf16[128]{0:T(256)(128)(2,1)S(1)}, bf16[128]{0:T(256)(128)(2,1)}, u32[]{:S(2)}) copy-start(bf16[128]{0:T(256)(128)(2,1)} %param.23) | copy-start | bytes 772
  113.9 61.9 %copy-start.2 = (bf16[4,16]{1,0:T(4,128)(2,1)S(1)}, bf16[4,16]{1,0:T(4,128)(2,1)}, u32[]{:S(2)}) copy-start(bf16[4,16]{1,0:T(4,128)(2,1)} %param.22) | copy-start | bytes 388
  113.9 121.8 %reduce-scatter.2.cloned.1.call-start = ((), (), s32[]{:S(2)}) async-start(), calls=%async_computation.2 | async-start | bytes 294912 | tf_op jit(solution)/shard_map/reduce_scatter | solution.py:135
Sparse Core Ops, SparseCore 0:
  9.5 37.1 all-gather.3
  114.1 49.0 all-gather.5
  175.9 59.7 reduce-scatter.1
where the time goes:
time: 265 us; the launch traced here: 264 us
  waiting for transfers between devices  145 us (55%)
  matrix products  66.4 us (25%)
  blocking collectives  19.4 us (7%)
  between operations  14 us (5%)
  local copies, waits for them, and re-layouts  9.67 us (4%)
  other arithmetic  8.34 us (3%)
    reduce_scatter x1, waiting for transfers between devices, per_device(): lax.psum_scatter(batched_f32(later_product, local_b), 'sp', scatter_dimen...  59.9 us
    all_gather x1, waiting for transfers between devices, prefix(): gathered = lax.all_gather(part, axis)  49.2 us
    all_gather x1, waiting for transfers between devices, per_device(): piece = lax.all_gather(tokens, 'tp', axis=1, tiled=True)  35.6 us
    psum x1, blocking collectives, per_device(): raw_read = lax.psum(partial_read, 'sp')  19.4 us
    dot_general x13, matrix products, matmul_f32(): return jnp.dot(left, right, precision=lax.Precision.HIGHEST)  18.7 us
    dot_general x8, matrix products, advance(): jnp.einsum('hcd,hce->hde', key_remainder, fresh, precision=lax.Precision....  13.2 us
    dot_general x8, matrix products, batched_f32(): jnp.einsum('hij,hjk->hik', left, right, precision=lax.Precision.HIGHEST)  12.2 us
    dot_general x8, matrix products, advance(): jnp.einsum('hcd,hde->hce', erase, state, precision=lax.Precision.HIGHEST)  10.7 us
  transfers between devices with their start and end apart: 3, of which 3 were waited for; matrix products, arithmetic and copies ran while one was open for 1% of the time, Pallas kernels for 0%

commit v1 on v0

--- a/solution.py
+++ b/solution.py
@@ -83,7 +83,12 @@
         ],
         axis=1,
     )
-    piece = lax.all_gather(tokens, "tp", axis=1, tiled=True)
+    ring = [tokens]
+    for hop in range(3):
+        ring.append(lax.ppermute(ring[-1], "tp", [(dev, (dev + 1) % 4) for dev in range(4)]))
+    piece = jnp.roll(
+        jnp.concatenate(ring[::-1], axis=1), (lax.axis_index("tp") + 1) * ring[0].shape[1], axis=1
+    )
     key_acc = jnp.dot(piece, w_key, preferred_element_type=jnp.float32)
     value_acc = jnp.dot(piece, w_value, preferred_element_type=jnp.float32)
     gate_acc = jnp.dot(piece, gate_weights, preferred_element_type=jnp.float32)

time: 265 us -> 271 us (1.023)
  waiting for transfers between devices: 145 us -> 152 us
  matrix products: 66.4 us -> 63.3 us
  local copies, waits for them, and re-layouts: 9.67 us -> 12.5 us
    ppermute x0 -> x3, waiting for transfers between devices: none -> 40.9 us  [per_device(): lax.ppermute(ring[-1], 'tp', [(dev, (dev + 1) % 4) for dev in range(4)])]
    all_gather x1 -> x0, waiting for transfers between devices: 35.6 us -> none  [per_device(): piece = lax.all_gather(tokens, 'tp', axis=1, tiled=True)]
    unnamed x11 -> x24, local copies, waits for them, and re-layouts: 0.11 us -> 8.84 us
    mul x8, local copies, waits for them, and re-layouts: 5.46 us -> 0.08 us  [advance(): keep[:, None, None] * state]
  transfers between devices with their start and end apart: 3 -> 5, of which waited for: 3 -> 5; matrix products, arithmetic and copies ran while one was open for 1% -> 1% of each run, Pallas kernels for 0% -> 0%
where the time goes in v1:
time: 271 us; the launch traced here: 270 us
  waiting for transfers between devices  152 us (56%)
  matrix products  63.3 us (23%)
  blocking collectives  19.5 us (7%)
  between operations  14.4 us (5%)
  local copies, waits for them, and re-layouts  12.5 us (5%)
  other arithmetic  6.52 us (2%)
    reduce_scatter x1, waiting for transfers between devices, per_device(): lax.psum_scatter(batched_f32(later_product, local_b), 'sp', scatter_dimen...  59.9 us
    all_gather x1, waiting for transfers between devices, prefix(): gathered = lax.all_gather(part, axis)  51.2 us
    ppermute x3, waiting for transfers between devices, per_device(): lax.ppermute(ring[-1], 'tp', [(dev, (dev + 1) % 4) for dev in range(4)])  40.9 us
    psum x1, blocking collectives, per_device(): raw_read = lax.psum(partial_read, 'sp')  19.5 us
    dot_general x13, matrix products, matmul_f32(): return jnp.dot(left, right, precision=lax.Precision.HIGHEST)  17.9 us
    dot_general x8, matrix products, advance(): jnp.einsum('hcd,hce->hde', key_remainder, fresh, precision=lax.Precision....  13.2 us
    dot_general x8, matrix products, batched_f32(): jnp.einsum('hij,hjk->hik', left, right, precision=lax.Precision.HIGHEST)  12.2 us
    dot_general x8, matrix products, advance(): jnp.einsum('hcd,hde->hce', erase, state, precision=lax.Precision.HIGHEST)  10.7 us
  transfers between devices with their start and end apart: 5, of which 5 were waited for; matrix products, arithmetic and copies ran while one was open for 1% of the time, Pallas kernels for 0%

profile of v1, /device:TPU:0, one launch (start us, length us, event | category | flops | bytes accessed | tf_op | source)
XLA Modules:
  0.0 269.6 jit_solution(5950774154429114380)
XLA Ops:
  7.8 14.6 %collective-permute-done = bf16[512,1024]{1,0:T(8,128)(2,1)S(1)} collective-permute-done((bf16[512,1024]{1,0:T(8,128)(2,1)}, bf16[512,1024]{1,0:T(8,128)(2,1)S(1)}, u32[]{:S(2)}, u32[]{:S(2)}) %collective-permute-start) | collective-permute-done | bytes 1048608 | tf_op jit(solution)/shard_map/ppermute | solution.py:88
  22.4 14.3 %collective-permute-done.1 = bf16[512,1024]{1,0:T(8,128)(2,1)} collective-permute-done((bf16[512,1024]{1,0:T(8,128)(2,1)S(1)}, bf16[512,1024]{1,0:T(8,128)(2,1)}, u32[]{:S(2)}, u32[]{:S(2)}) %collective-permute-start.1) | collective-permute-done | bytes 1048608 | tf_op jit(solution)/shard_map/ppermute | solution.py:88
  39.3 11.9 %collective-permute-done.2 = bf16[512,1024]{1,0:T(8,128)(2,1)} collective-permute-done((bf16[512,1024]{1,0:T(8,128)(2,1)}, bf16[512,1024]{1,0:T(8,128)(2,1)}, u32[]{:S(2)}, u32[]{:S(2)}) %collective-permute-start.2) | collective-permute-done | bytes 1048608 | tf_op jit(solution)/shard_map/ppermute | solution.py:88
  57.0 3.2 %copy-done.1 = bf16[512,8192]{1,0:T(8,128)(2,1)} copy-done((bf16[512,8192]{1,0:T(8,128)(2,1)}, bf16[512,8192]{1,0:T(8,128)(2,1)S(1)}, u32[]{:S(2)}) %copy-start.1) | copy-done | bytes 8388632
  62.8 5.8 %fusion.24 = bf16[512,512]{1,0:T(8,128)(2,1)S(1)} fusion(bf16[4096,512]{1,0:T(8,128)(2,1)} %param.15, bf16[512,8192]{1,0:T(8,128)(2,1)} %copy-done.1, s32[]{:T(128)S(6)} %select_n.42), kind=kOutput, calls=%fused_computation.29 | convolution fusion | flops 2147745792 | bytes 8912900 | tf_op jit(solution)/shard_map/dot_general | solution.py:92
  70.2 1.9 fusion.21
  79.4 1.4 fusion.33
  83.2 2.3 fusion.27
  86.9 2.6 convolution_bitcast_fusion.1
  92.1 24.5 %while.22 = (s32[]{:T(128)}, f32[4,128,256]{2,1,0:T(8,128)S(1)}, f32[8,4]{1,0:T(8,128)S(1)}, f32[8,4,64,128]{3,2,0,1:T(8,128)}, f32[8,4,64,128]{3,2,0,1:T(8,128)S(1)}, /*index=5*/f32[8,4,64,128]{3,2,0,1:T(8,128)}, s32[]{:T(128)}) while((s32[]{:T(128)}, f32[4,128,256]{2,1,0:T(8,128)S(1)}, f32[8,4]{1,0:T(8,128)S(1)}, ...), condition=%wide.region_3.4_spmd, body=%wide.region_2.3_spmd.sunk | while | flops 201654272 | bytes 2753669 | solution.py:136
  92.1 1.3 convolution_subtract_fusion.2
  93.4 1.7 convolution_add_fusion.3
  96.5 1.7 convolution_add_fusion.3
  98.2 1.3 convolution_subtract_fusion.2
  99.6 1.7 convolution_add_fusion.3
  102.6 1.7 convolution_add_fusion.3
  105.7 1.7 convolution_add_fusion.3
  108.7 1.7 convolution_add_fusion.3
  111.8 1.7 convolution_add_fusion.3
  114.9 1.7 convolution_add_fusion.3
  117.3 51.2 %all-gather.3.cloned.1.call-done = f32[32,128,128]{2,1,0:T(8,128)} async-done(((f32[4,128,128]{2,1,0:T(8,128)}), f32[32,128,128]{2,1,0:T(8,128)}) %all-gather.3.cloned.1.call-update) | async-done | bytes 2097168 | tf_op jit(solution)/shard_map/all_gather | solution.py:16
  168.6 11.3 %while.23 = (s32[]{:T(128)}, f32[4,128,128]{1,2,0:T(8,128)S(1)}, s32[]{:T(128)}, f32[8,4,128,128]{3,2,1,0:T(8,128)}, s32[]{:T(128)}, /*index=5*/s32[]{:T(128)}, s32[]{:T(128)}, s32[]{:T(128)}) while((s32[]{:T(128)}, f32[4,128,128]{1,2,0:T(8,128)S(1)}, s32[]{:T(128)}, f32[8,4,128,128]{3,2,1,0:T(8,128)}, s32[]{:T(128)}, /*index=5*/s32[]{:T(128)}, ...), condition=%wide.region_5.6_spmd, body=%wide.region_4.5_spmd.sunk | while | flops 100663304 | bytes 1310855 | solution.py:23
  168.6 1.6 convolution_bitcast_fusion.4
  170.3 1.6 convolution_bitcast_fusion.4
  171.9 1.6 convolution_bitcast_fusion.4
  173.5 1.6 convolution_bitcast_fusion.4
  175.1 1.6 convolution_bitcast_fusion.4
  176.7 1.6 convolution_bitcast_fusion.4
  178.3 1.6 convolution_bitcast_fusion.4
  181.3 59.9 %reduce-scatter.2.cloned.1.call-done = f32[4,16,128]{2,1,0:T(8,128)} async-done(((f32[4,128,128]{2,1,0:T(8,128)}), f32[4,16,128]{2,1,0:T(8,128)}) %reduce-scatter.2.cloned.1.call-update) | async-done | bytes 32784 | tf_op jit(solution)/shard_map/reduce_scatter | solution.py:140
  241.1 1.4 multiply_reduce_fusion.1
  242.5 19.5 %psum.7 = f32[4,128]{1,0:T(4,128)S(1)} all-reduce(f32[4,128]{1,0:T(4,128)S(1)} %get-tuple-element.144), channel_id=1, replica_groups=mesh['sp'=8,'tp'=4] {'sp'}, use_global_device_ids=true, to_apply=%region_8.9 | all-reduce | flops 512 | bytes 4096 | tf_op jit(solution)/shard_map/psum | solution.py:147
  (104 shorter events, 37.7 us)
Async XLA Ops:
  7.2 46.9 %copy-start = (bf16[512,1024]{1,0:T(8,128)(2,1)S(1)}, bf16[512,1024]{1,0:T(8,128)(2,1)}, u32[]{:S(2)}) copy-start(bf16[512,1024]{1,0:T(8,128)(2,1)} %param.14) | copy-start | bytes 3145732
  7.2 161.4 %all-gather.3.cloned.1.call-start = ((), (), s32[]{:S(2)}) async-start(), calls=%async_computation.2 | async-start | bytes 2359296 | tf_op jit(solution)/shard_map/all_gather | solution.py:16
  7.2 15.2 %collective-permute-start = (bf16[512,1024]{1,0:T(8,128)(2,1)}, bf16[512,1024]{1,0:T(8,128)(2,1)S(1)}, u32[]{:S(2)}, u32[]{:S(2)}) collective-permute-start(bf16[512,1024]{1,0:T(8,128)(2,1)} %param.14), channel_id=1, source_target_pairs={{0,1},{1,2},{2,3},{3,0},{4,5},{5,6},{6,7},{7,4},{8,9},{9,10},{10,1... | collective-permute-start | bytes 3145736 | tf_op jit(solution)/shard_map/ppermute | solution.py:88
  22.4 14.3 %collective-permute-start.1 = (bf16[512,1024]{1,0:T(8,128)(2,1)S(1)}, bf16[512,1024]{1,0:T(8,128)(2,1)}, u32[]{:S(2)}, u32[]{:S(2)}) collective-permute-start(bf16[512,1024]{1,0:T(8,128)(2,1)S(1)} %collective-permute-done), channel_id=1, source_target_pairs={{0,1},{1,2},{2,3},{3,0},{4,5},{5,6},{6,7},{7,4},{8,9},{9,10},{10,1... | collective-permute-start | bytes 3145736 | tf_op jit(solution)/shard_map/ppermute | solution.py:88
  36.7 14.5 %collective-permute-start.2 = (bf16[512,1024]{1,0:T(8,128)(2,1)}, bf16[512,1024]{1,0:T(8,128)(2,1)}, u32[]{:S(2)}, u32[]{:S(2)}) collective-permute-start(bf16[512,1024]{1,0:T(8,128)(2,1)} %collective-permute-done.1), channel_id=1, source_target_pairs={{0,1},{1,2},{2,3},{3,0},{4,5},{5,6},{6,7},{7,4},{8,9},{9,10},{10,1... | collective-permute-start | bytes 3145736 | tf_op jit(solution)/shard_map/ppermute | solution.py:88
  53.9 7.4 %copy-start.2 = (f32[4,512]{1,0:T(4,128)S(1)}, f32[4,512]{1,0:T(4,128)}, u32[]{:S(2)}) copy-start(f32[4,512]{1,0:T(4,128)} %param.21) | copy-start | bytes 24580
  56.9 3.2 %copy-start.1 = (bf16[512,8192]{1,0:T(8,128)(2,1)}, bf16[512,8192]{1,0:T(8,128)(2,1)S(1)}, u32[]{:S(2)}) copy-start(bf16[512,8192]{1,0:T(8,128)(2,1)S(1)} %constant_dynamic-update-slice_fusion) | copy-start | bytes 25165828
  77.0 6.2 %slice-start = ((s8[8388608]{0:T(1024)(128)(4,1)}), s8[4194304]{0:T(1024)(128)(4,1)S(1)}, s32[]{:S(2)}) async-start(s8[8388608]{0:T(1024)(128)(4,1)} %bitcast.100), calls=%async_computation.3 | async-start | bytes 8388608
  77.0 6.2 %copy-start.4 = (bf16[4096,512]{1,0:T(8,128)(2,1)S(1)}, bf16[4096,512]{1,0:T(8,128)(2,1)}, u32[]{:S(2)}) copy-start(bf16[4096,512]{1,0:T(8,128)(2,1)} %param.16) | copy-start | bytes 12582916
  79.4 3.8 %slice-start.1 = ((s8[8388608]{0:T(1024)(128)(4,1)}), s8[4194304]{0:T(1024)(128)(4,1)S(1)}, s32[]{:S(2)}) async-start(s8[8388608]{0:T(1024)(128)(4,1)} %bitcast.100), calls=%async_computation.4 | async-start | bytes 8388608
  92.1 89.2 %copy-start.3 = (bf16[4,16]{1,0:T(4,128)(2,1)S(1)}, bf16[4,16]{1,0:T(4,128)(2,1)}, u32[]{:S(2)}) copy-start(bf16[4,16]{1,0:T(4,128)(2,1)} %param.22) | copy-start | bytes 388
  92.1 89.2 %copy-start.5 = (bf16[128]{0:T(256)(128)(2,1)S(1)}, bf16[128]{0:T(256)(128)(2,1)}, u32[]{:S(2)}) copy-start(bf16[128]{0:T(256)(128)(2,1)} %param.23) | copy-start | bytes 772
  117.3 123.8 %reduce-scatter.2.cloned.1.call-start = ((), (), s32[]{:S(2)}) async-start(), calls=%async_computation.1 | async-start | bytes 294912 | tf_op jit(solution)/shard_map/reduce_scatter | solution.py:140
Sparse Core Ops, SparseCore 0:
  117.4 51.1 all-gather.2
  181.3 59.7 reduce-scatter.1
